TPU v7x, 256 devices: a whole 4x4x8 slice. The times are simulated.
256 devices in a mesh: sp: 32 (over z, x), tp: 8 (over y, core).
Axes of the slice: x: 4, y: 4, z: 8, core: 2. Of those that a mesh axis runs over, the one named last changes fastest.
Arguments:
- tokens: bfloat16 [16384, 2048], P(('sp', 'tp')), may hold values from -64 to 64
- query_weight: bfloat16 [2048, 2048], P(None, 'tp'), may hold values from -0.125 to 0.125
- key_weight: bfloat16 [2048, 2048], P(None, 'tp'), may hold values from -0.125 to 0.125
- value_weight: bfloat16 [2048, 2048], P(None, 'tp'), may hold values from -0.125 to 0.125
- gate_weight: bfloat16 [2048, 2048], P(None, 'tp'), may hold values from -0.125 to 0.125
- forget_weight: bfloat16 [2048, 16], replicated, may hold values from -0.125 to 0.125
- forget_bias: float32 [16], replicated, as said below
- out_weight: bfloat16 [2048, 2048], replicated, may hold values from -0.125 to 0.125
Outputs:
- mixed: bfloat16 [16384, 2048], P(('sp', 'tp'))
Inputs may be any that keep to these rules, and one draw needn't show every extreme that they name: `forget_bias`: every head's forget bias is at least 4.
All inputs are finite; a program needn't handle non-finite values.
Results may differ from a plain program's by a relative error of at most 0.015.
The roundings to bfloat16 on the way count: a program that leaves them out, or rounds other values in their place, can miss the bound.
Values may be sent and summed in bfloat16 or wider, within the bound.
No kernel may reach another device: no remote copies, remote signals or barrier semaphores. Data moves between devices by JAX's collectives and lax.ppermute only.
A program may use at most 128 MiB of HBM per device.

v0:
```python
import math
import jax
import jax.numpy as jnp
from jax import lax
from jax.sharding import PartitionSpec as P

HEAD_DIM = 128


def body(
    tokens,
    query_weight,
    key_weight,
    value_weight,
    gate_weight,
    forget_weight,
    forget_bias,
    out_weight,
):
    width = query_weight.shape[1]
    heads_dev = width // HEAD_DIM
    first_head = lax.axis_index("tp") * heads_dev
    piece = lax.all_gather(tokens, "tp", axis=0, tiled=True)
    products = [
        jnp.dot(piece, weight, preferred_element_type=jnp.float32)
        for weight in (query_weight, key_weight, value_weight, gate_weight, forget_weight)
    ]
    joined = jnp.concatenate(products, axis=1)
    rows = joined.shape[0]
    queries = (
        (joined[:, :width] * HEAD_DIM ** (-0.5))
        .astype(jnp.bfloat16)
        .reshape(rows, heads_dev, HEAD_DIM)
    )
    keys = joined[:, width : 2 * width].astype(jnp.bfloat16)
    values = joined[:, 2 * width : 3 * width].astype(jnp.bfloat16)
    gate = jax.nn.sigmoid(joined[:, 3 * width : 4 * width])
    logits = lax.dynamic_slice_in_dim(joined[:, 4 * width :], first_head, heads_dev, 1)
    bias = lax.dynamic_slice_in_dim(forget_bias, first_head, heads_dev, 0)
    forget_log = jax.nn.log_sigmoid(logits + bias).T
    all_logs = lax.all_gather(forget_log, "sp", axis=1, tiled=True)
    cumul = jnp.cumsum(all_logs, axis=1)
    my_start = lax.axis_index("sp") * rows
    last_query = my_start + rows - 1
    cum_query = lax.dynamic_slice_in_dim(cumul, my_start, rows, 1)
    query_pos = my_start + jnp.arange(rows, dtype=jnp.int32)
    paired = jnp.stack([keys, values])

    def absorb(carry, key_blk, value_blk, key_start):
        best, total, accum = carry
        span = key_blk.shape[0]
        scores = jnp.einsum(
            "qhd,khd->hqk",
            queries,
            key_blk.reshape(span, heads_dev, HEAD_DIM),
            preferred_element_type=jnp.float32,
        )
        cum_key = lax.dynamic_slice_in_dim(cumul, jnp.maximum(key_start, 0), span, 1)
        scores = scores + cum_query[:, :, None] - cum_key[:, None, :]
        key_pos = key_start + jnp.arange(span, dtype=jnp.int32)
        valid = (key_pos[None, :] <= query_pos[:, None]) & (key_pos[None, :] >= 0)
        scores = jnp.where(valid[None], scores, -jnp.inf)
        new_best = jnp.maximum(best, jnp.max(scores, axis=-1))
        factor = jnp.exp(best - new_best)
        weights = jnp.exp(scores - new_best[..., None])
        total = total * factor + jnp.sum(weights, axis=-1)
        accum = accum * factor[..., None] + jnp.einsum(
            "hqk,khd->hqd",
            weights.astype(jnp.bfloat16),
            value_blk.reshape(span, heads_dev, HEAD_DIM),
            preferred_element_type=jnp.float32,
        )
        return (new_best, total, accum)

    initial = (
        jnp.full((heads_dev, rows), -1e30, jnp.float32),
        jnp.zeros((heads_dev, rows), jnp.float32),
        jnp.zeros((heads_dev, rows, HEAD_DIM), jnp.float32),
    )
    carry = initial
    piece = lax.all_gather(paired, "sp", axis=1, tiled=True)
    length = piece.shape[1]
    span = math.gcd(length, 512)
    steps = length // span
    key_blocks = piece[0].reshape(steps, span, width)
    value_blocks = piece[1].reshape(steps, span, width)
    offsets = jnp.arange(steps, dtype=jnp.int32) * span

    def one(state, inputs):
        state = lax.cond(
            inputs[2] <= last_query,
            lambda inner: absorb(inner, inputs[0], inputs[1], inputs[2]),
            lambda inner: inner,
            state,
        )
        return (state, None)

    carry, _ = lax.scan(one, carry, (key_blocks, value_blocks, offsets))
    best, total, accum = carry
    heads_out = (accum / total[..., None]).transpose(1, 0, 2).reshape(rows, width)
    attended = (heads_out * gate).astype(jnp.bfloat16)
    own_rows = lax.dynamic_slice_in_dim(out_weight, first_head * HEAD_DIM, width, 0)
    mixed = lax.psum_scatter(
        jnp.dot(attended, own_rows, preferred_element_type=jnp.float32).astype(jnp.bfloat16),
        "tp",
        scatter_dimension=0,
        tiled=True,
    )
    return mixed


def solution(mesh):
    placed = (
        P(("sp", "tp"), None),
        P(None, "tp"),
        P(None, "tp"),
        P(None, "tp"),
        P(None, "tp"),
        P(),
        P(),
        P(),
    )
    return jax.shard_map(
        body, mesh=mesh, in_specs=placed, out_specs=P(("sp", "tp"), None), check_vma=False
    )
```

profile of v0, /device:TPU:2, one launch (start us, length us, event | category | flops | bytes accessed | tf_op | source)
XLA Modules:
  0.0 454.7 jit_solution(7296809608910442630)
XLA Ops:
  6.5 0.7 all-gather.3.cloned.1.call-update
  7.3 32.7 %all-gather.3.cloned.1.call-done = bf16[512,2048]{1,0:T(8,128)(2,1)} async-done(((bf16[64,2048]{1,0:T(8,128)(2,1)}), bf16[512,2048]{1,0:T(8,128)(2,1)}) %all-gather.3.cloned.1.call-update) | async-done | bytes 2097168 | tf_op jit(solution)/shard_map/all_gather | solution.py:23
  40.1 2.7 fusion.12
  42.9 0.7 fusion.13
  43.6 0.9 pad_maximum_fusion
  44.6 0.6 fusion.22
  45.4 43.4 %all_gather.11 = f32[2,16384]{1,0:T(2,128)S(1)} all-gather(f32[2,512]{1,0:T(2,128)S(1)} %fusion.17), channel_id=1, replica_groups=mesh['sp'=32,'tp'=8] {'sp'}, dimensions={1}, use_global_device_ids=true | all-gather | bytes 135168 | tf_op jit(solution)/shard_map/all_gather | solution.py:41
  89.7 2.0 fusion.11
  91.9 91.9 %all-gather.5.cloned.1.call-done = bf16[2,16384,256]{2,1,0:T(8,128)(2,1)} async-done(((bf16[2,512,256]{2,1,0:T(8,128)(2,1)}), bf16[2,16384,256]{2,1,0:T(8,128)(2,1)}) %all-gather.5.cloned.1.call-update) | async-done | bytes 16777232 | tf_op jit(solution)/shard_map/all_gather | solution.py:81
  183.8 11.3 %fusion.21 = (bf16[1,16384,256]{2,1,0:T(8,128)(2,1)}, bf16[1,16384,256]{2,1,0:T(8,128)(2,1)}) fusion(bf16[2,16384,256]{2,1,0:T(8,128)(2,1)} %all-gather.5.cloned.1.call-done), kind=kLoop, calls=%fused_computation.44 | loop fusion | bytes 33554432 | tf_op jit(solution)/shard_map/slice | solution.py:86
  195.0 12.0 %copy.17 = bf16[32,512,256]{1,2,0:T(8,128)(2,1)} copy(bf16[32,512,256]{2,1,0:T(8,128)(2,1)} %bitcast.42) | data formatting | bytes 16777216
  207.1 11.9 %copy.19 = bf16[32,512,256]{1,2,0:T(8,128)(2,1)} copy(bf16[32,512,256]{2,1,0:T(8,128)(2,1)} %bitcast.41) | data formatting | bytes 16777216
  219.0 46.5 %while.15 = (s32[]{:T(128)}, f32[2,512]{1,0:T(2,128)S(1)}, f32[2,512]{1,0:T(2,128)S(1)}, f32[2,512,128]{2,1,0:T(8,128)S(1)}, s32[32]{0:T(128)S(1)}, /*index=5*/s...) while((s32[]{:T(128)}, f32[2,512]{1,0:T(2,128)S(1)}, ...), condition=%wide.region_7.8_spmd.clone, body=%wide.region_2.7_spmd.clone.sunk | while | flops 273420288 | bytes 9794895 | solution.py:98
  219.0 0.6 dynamic_slice.51
  220.1 4.8 %conditional.3 = ((f32[2,512]{1,0:T(2,128)S(1)}, f32[2,512]{1,0:T(2,128)S(1)}, f32[2,512,128]{2,1,0:T(8,128)S(1)})) conditional(s32[]{:T(128)} %convert_element_type.43, (f32[2,512]{1,0:T(2,128)S(1)}, f32[2,512]{1,0:T(2,128)S(1)}, f32[2,512,128]{2,1,0:T(8,128)S(1)}) %tuple.43, (s32[]{:T(128)}, s32[]{:T(128)}, bf16[32,512,256]{1,2,0:T(8,128)(2,1)}, ...), branch_computations={%region_3.3_spmd, %region_4.6_spmd} | conditional | flops 273420288 | bytes 9792576 | solution.py:90
  222.1 1.1 constant_dynamic-slice_fusion
  223.2 0.7 fusion.20
  224.2 0.7 convolution_add_fusion
  225.0 0.6 dynamic_slice.51
  226.1 4.9 %conditional.3 = ((f32[2,512]{1,0:T(2,128)S(1)}, f32[2,512]{1,0:T(2,128)S(1)}, f32[2,512,128]{2,1,0:T(8,128)S(1)})) conditional(s32[]{:T(128)} %convert_element_type.43, (f32[2,512]{1,0:T(2,128)S(1)}, f32[2,512]{1,0:T(2,128)S(1)}, f32[2,512,128]{2,1,0:T(8,128)S(1)}) %tuple.43, (s32[]{:T(128)}, s32[]{:T(128)}, bf16[32,512,256]{1,2,0:T(8,128)(2,1)}, ...), branch_computations={%region_3.3_spmd, %region_4.6_spmd} | conditional | flops 273420288 | bytes 9792576 | solution.py:90
  228.1 1.1 constant_dynamic-slice_fusion
  229.2 0.7 fusion.20
  230.2 0.7 convolution_add_fusion
  232.1 0.6 dynamic_slice.51
  233.3 0.6 dynamic_slice.51
  235.6 0.6 dynamic_slice.51
  236.7 0.6 dynamic_slice.51
  239.0 0.6 dynamic_slice.51
  240.2 0.6 dynamic_slice.51
  241.3 0.6 dynamic_slice.51
  242.5 0.6 dynamic_slice.51
  243.6 0.6 dynamic_slice.51
  244.8 0.6 dynamic_slice.51
  245.9 0.6 dynamic_slice.51
  247.1 0.6 dynamic_slice.51
  248.2 0.6 dynamic_slice.51
  250.5 0.6 dynamic_slice.51
  251.7 0.6 dynamic_slice.51
  254.0 0.6 dynamic_slice.51
  255.1 0.6 dynamic_slice.51
  257.4 0.6 dynamic_slice.51
  258.6 0.6 dynamic_slice.51
  260.9 0.6 dynamic_slice.51
  262.0 0.6 dynamic_slice.51
  263.2 0.6 dynamic_slice.51
  264.3 0.6 dynamic_slice.51
  265.8 4.8 %convolution_convert_fusion = bf16[512,2048]{1,0:T(8,128)(2,1)} fusion(f32[512,256]{0,1:T(8,128)S(1)} %bitcast.45, bf16[512,2048]{1,0:T(8,128)(2,1)} %all-gather.3.cloned.1.call-done, bf16[2048,256]{1,0:T(8,128)(2,1)S(1)} %copy-done, bf16[2048,2048]{1,0:T(8,128)(2,1)} %param.19, s32[]{:T(128)S(6)} %select_n.25), kind=kOutput, calls=%fused_computation.16 | convolution fusion | flops 1075445760 | bytes 6815748 | tf_op jit(solution)/shard_map/dot_general | solution.py:104
  270.6 177.6 %reduce-scatter.2.cloned.1.call-done = bf16[64,2048]{1,0:T(8,128)(2,1)} async-done(((bf16[512,2048]{1,0:T(8,128)(2,1)}), bf16[64,2048]{1,0:T(8,128)(2,1)}) %reduce-scatter.2.cloned.1.call-update) | async-done | bytes 262160 | tf_op jit(solution)/shard_map/reduce_scatter | solution.py:103
  (119 shorter events, 9.6 us)
Async XLA Ops:
  6.5 259.2 %copy-start = (bf16[2048,256]{1,0:T(8,128)(2,1)S(1)}, bf16[2048,256]{1,0:T(8,128)(2,1)}, u32[]{:S(2)}) copy-start(bf16[2048,256]{1,0:T(8,128)(2,1)} %param.16) | copy-start | bytes 3145732
  6.5 33.5 %all-gather.3.cloned.1.call-start = ((), (), s32[]{:S(2)}) async-start(), calls=%async_computation.1 | async-start | bytes 2359296 | tf_op jit(solution)/shard_map/all_gather | solution.py:23
  7.3 176.5 %all-gather.5.cloned.1.call-start = ((), (), s32[]{:S(2)}) async-start(), calls=%async_computation.2 | async-start | bytes 17301504 | tf_op jit(solution)/shard_map/all_gather | solution.py:81
  40.1 2.7 copy-start.1
  40.1 2.8 copy-start.3
  42.9 1.7 copy-start.4
  42.9 1.8 copy-start.2
  44.5 403.7 %reduce-scatter.2.cloned.1.call-start = ((), (), s32[]{:S(2)}) async-start(), calls=%async_computation.3 | async-start | bytes 2359296 | tf_op jit(solution)/shard_map/reduce_scatter | solution.py:103
Sparse Core Ops, SparseCore 0:
  9.2 30.8 all-gather.2
  44.6 139.1 all-gather.4
  270.7 177.4 reduce-scatter.1
where the time goes:
time: 457 us; the launch traced here: 455 us
  waiting for transfers between devices  303 us (66%)
  local copies, waits for them, and re-layouts  56.2 us (12%)
  blocking collectives  43.4 us (9%)
  loops' own time  20.2 us (4%)
  matrix products  13.7 us (3%)
  between operations  13.3 us (3%)
  other arithmetic  4.91 us (1%)
    reduce_scatter x1, waiting for transfers between devices, body(): lax.psum_scatter(jnp.dot(attended, own_rows, preferred_element_type=jnp.f...  178 us
    all_gather x1, waiting for transfers between devices, body(): piece = lax.all_gather(paired, 'sp', axis=1, tiled=True)  91.9 us
    all_gather x1, blocking collectives, body(): all_logs = lax.all_gather(forget_log, 'sp', axis=1, tiled=True)  43.4 us
    all_gather x1, waiting for transfers between devices, body(): piece = lax.all_gather(tokens, 'tp', axis=0, tiled=True)  32.7 us
    unnamed x15, local copies, waits for them, and re-layouts  24.2 us
    dynamic_slice x34, local copies, waits for them, and re-layouts, body(): carry, _ = lax.scan(one, carry, (key_blocks, value_blocks, offsets))  19.9 us
    another operation x1, loops' own time, body(): carry, _ = lax.scan(one, carry, (key_blocks, value_blocks, offsets))  18.5 us
    slice x1, local copies, waits for them, and re-layouts, body(): value_blocks = piece[1].reshape(steps, span, width)  11.3 us
  transfers between devices with their start and end apart: 3, of which 3 were waited for; matrix products, arithmetic and copies ran while one was open for 1% of the time, Pallas kernels for 0%

commit v1 on v0

--- a/solution.py
+++ b/solution.py
@@ -78,7 +78,8 @@
         jnp.zeros((heads_dev, rows, HEAD_DIM), jnp.float32),
     )
     carry = initial
-    piece = lax.all_gather(paired, "sp", axis=1, tiled=True)
+    shards = lax.all_gather(paired, "sp", axis=0, tiled=False)
+    piece = jnp.concatenate(shards, axis=1)
     length = piece.shape[1]
     span = math.gcd(length, 512)
     steps = length // span

time: 457 us -> 471 us (1.031)
  waiting for transfers between devices: 303 us -> 310 us
    unnamed x15, local copies, waits for them, and re-layouts: 24.2 us -> 0.38 us
    all_gather x0 -> x1, local copies, waits for them, and re-layouts: none -> 21.3 us  [body(): shards = lax.all_gather(paired, 'sp', axis=0, tiled=False)]
    another operation x2 -> x3, local copies, waits for them, and re-layouts: 0.1 us -> 11.5 us  [the longest x1 11.4 us: body(): value_blocks = piece[1].reshape(steps, span, width)]
    slice x2 -> x1, local copies, waits for them, and re-layouts: 11.3 us -> 0.01 us  [the longest x1 11.3 us: body(): value_blocks = piece[1].reshape(steps, span, width)]
    reduce_scatter x1, waiting for transfers between devices: 178 us -> 185 us  [body(): lax.psum_scatter(jnp.dot(attended, own_rows, preferred_element_type=jnp.f...]
where the time goes in v1:
time: 471 us; the launch traced here: 469 us
  waiting for transfers between devices  310 us (66%)
  local copies, waits for them, and re-layouts  57.9 us (12%)
  blocking collectives  43.5 us (9%)
  loops' own time  22.8 us (5%)
  matrix products  13.9 us (3%)
  between operations  13.2 us (3%)
  other arithmetic  7.21 us (2%)
    reduce_scatter x1, waiting for transfers between devices, body(): lax.psum_scatter(jnp.dot(attended, own_rows, preferred_element_type=jnp.f...  185 us
    all_gather x1, waiting for transfers between devices, body(): shards = lax.all_gather(paired, 'sp', axis=0, tiled=False)  92 us
    all_gather x1, blocking collectives, body(): all_logs = lax.all_gather(forget_log, 'sp', axis=1, tiled=True)  43.5 us
    all_gather x1, waiting for transfers between devices, body(): piece = lax.all_gather(tokens, 'tp', axis=0, tiled=True)  32.7 us
    all_gather x1, local copies, waits for them, and re-layouts, body(): shards = lax.all_gather(paired, 'sp', axis=0, tiled=False)  21.3 us
    dynamic_slice x34, local copies, waits for them, and re-layouts, body(): carry, _ = lax.scan(one, carry, (key_blocks, value_blocks, offsets))  21.2 us
    another operation x1, loops' own time, body(): carry, _ = lax.scan(one, carry, (key_blocks, value_blocks, offsets))  21 us
    another operation x1, local copies, waits for them, and re-layouts, body(): value_blocks = piece[1].reshape(steps, span, width)  11.4 us
  transfers between devices with their start and end apart: 3, of which 3 were waited for; matrix products, arithmetic and copies ran while one was open for 1% of the time, Pallas kernels for 0%

profile of v1, /device:TPU:2, one launch (start us, length us, event | category | flops | bytes accessed | tf_op | source)
XLA Modules:
  0.0 468.7 jit_solution(3085917844232883580)
XLA Ops:
  6.5 0.7 all-gather.4.cloned.1.call-update
  7.3 32.7 %all-gather.4.cloned.1.call-done = bf16[512,2048]{1,0:T(8,128)(2,1)} async-done(((bf16[64,2048]{1,0:T(8,128)(2,1)}), bf16[512,2048]{1,0:T(8,128)(2,1)}) %all-gather.4.cloned.1.call-update) | async-done | bytes 2097168 | tf_op jit(solution)/shard_map/all_gather | solution.py:23
  40.1 2.7 fusion.12
  42.9 0.7 fusion.13
  43.6 0.9 pad_maximum_fusion
  44.6 0.6 fusion.21
  45.4 43.5 %all_gather.15 = f32[2,16384]{1,0:T(2,128)S(1)} all-gather(f32[2,512]{1,0:T(2,128)S(1)} %fusion.17), channel_id=1, replica_groups=mesh['sp'=32,'tp'=8] {'sp'}, dimensions={1}, use_global_device_ids=true | all-gather | bytes 135168 | tf_op jit(solution)/shard_map/all_gather | solution.py:41
  89.7 2.0 fusion.11
  91.9 92.0 %all-gather.6.cloned.1.call-done = bf16[64,512,256]{2,1,0:T(8,128)(2,1)} async-done(((bf16[2,512,256]{2,1,0:T(8,128)(2,1)}), bf16[64,512,256]{2,1,0:T(8,128)(2,1)}) %all-gather.6.cloned.1.call-update) | async-done | bytes 16777232 | tf_op jit(solution)/shard_map/all_gather | solution.py:81
  184.0 21.3 %copy.24 = bf16[32,2,512,256]{2,3,0,1:T(8,128)(2,1)} copy(bf16[32,2,512,256]{3,2,1,0:T(8,128)(2,1)} %bitcast.47) | data formatting | bytes 33554432 | tf_op jit(solution)/shard_map/all_gather | solution.py:81
  205.2 11.4 %slice_bitcast_fusion = (bf16[32,512,256]{1,2,0:T(8,128)(2,1)}, bf16[32,512,256]{1,2,0:T(8,128)(2,1)}) fusion(bf16[2,32,512,256]{2,3,1,0:T(8,128)(2,1)} %bitcast.45), kind=kLoop, calls=%fused_computation.16 | loop fusion | bytes 33554432 | tf_op jit(solution)/shard_map/reshape;squeeze | solution.py:87
  216.7 50.7 %while.15 = (s32[]{:T(128)}, f32[2,512]{1,0:T(2,128)S(1)}, f32[2,512]{1,0:T(2,128)S(1)}, f32[2,512,128]{2,1,0:T(8,128)S(1)}, s32[32]{0:T(128)S(1)}, /*index=5*/s...) while((s32[]{:T(128)}, f32[2,512]{1,0:T(2,128)S(1)}, ...), condition=%wide.region_7.8_spmd.clone, body=%wide.region_2.7_spmd.clone.sunk | while | flops 273420288 | bytes 9794895 | solution.py:99
  216.7 0.6 dynamic_slice.51
  218.0 5.1 %conditional.3 = ((f32[2,512]{1,0:T(2,128)S(1)}, f32[2,512]{1,0:T(2,128)S(1)}, f32[2,512,128]{2,1,0:T(8,128)S(1)})) conditional(s32[]{:T(128)} %convert_element_type.43, (f32[2,512]{1,0:T(2,128)S(1)}, f32[2,512]{1,0:T(2,128)S(1)}, f32[2,512,128]{2,1,0:T(8,128)S(1)}) %tuple.44, (s32[]{:T(128)}, s32[]{:T(128)}, bf16[32,512,256]{1,2,0:T(8,128)(2,1)}, ...), branch_computations={%region_3.3_spmd, %region_4.6_spmd} | conditional | flops 273420288 | bytes 9792576 | solution.py:91
  218.0 0.6 iota_add_fusion
  218.6 0.6 broadcast_compare_fusion
  220.2 1.1 constant_dynamic-slice_fusion
  221.3 0.7 fusion.20
  222.3 0.7 convolution_add_fusion
  223.1 0.6 dynamic_slice.51
  224.3 5.1 %conditional.3 = ((f32[2,512]{1,0:T(2,128)S(1)}, f32[2,512]{1,0:T(2,128)S(1)}, f32[2,512,128]{2,1,0:T(8,128)S(1)})) conditional(s32[]{:T(128)} %convert_element_type.43, (f32[2,512]{1,0:T(2,128)S(1)}, f32[2,512]{1,0:T(2,128)S(1)}, f32[2,512,128]{2,1,0:T(8,128)S(1)}) %tuple.44, (s32[]{:T(128)}, s32[]{:T(128)}, bf16[32,512,256]{1,2,0:T(8,128)(2,1)}, ...), branch_computations={%region_3.3_spmd, %region_4.6_spmd} | conditional | flops 273420288 | bytes 9792576 | solution.py:91
  224.3 0.6 iota_add_fusion
  225.0 0.6 broadcast_compare_fusion
  226.5 1.1 constant_dynamic-slice_fusion
  227.6 0.7 fusion.20
  228.7 0.7 convolution_add_fusion
  229.4 0.6 dynamic_slice.51
  230.7 0.6 dynamic_slice.51
  231.9 0.6 dynamic_slice.51
  233.2 0.6 dynamic_slice.51
  234.5 0.6 dynamic_slice.51
  235.7 0.6 dynamic_slice.51
  237.0 0.6 dynamic_slice.51
  239.6 0.6 dynamic_slice.51
  240.8 0.6 dynamic_slice.51
  244.6 0.6 dynamic_slice.51
  245.9 0.6 dynamic_slice.51
  249.7 0.6 dynamic_slice.51
  251.0 0.6 dynamic_slice.51
  254.8 0.6 dynamic_slice.51
  259.8 0.6 dynamic_slice.51
  263.6 0.6 dynamic_slice.51
  264.9 0.6 dynamic_slice.51
  267.4 1.0 copy.28
  268.4 2.1 broadcast_divide_fusion
  270.5 2.0 copy.29
  272.6 5.0 %convolution_convert_fusion = bf16[512,2048]{1,0:T(8,128)(2,1)} fusion(f32[512,256]{1,0:T(8,128)} %copy.29, bf16[512,2048]{1,0:T(8,128)(2,1)S(1)} %copy-done.2, bf16[2048,256]{1,0:T(8,128)(2,1)S(1)} %copy-done, bf16[2048,2048]{1,0:T(8,128)(2,1)} %param.19, s32[]{:T(128)S(6)} %select_n.25), kind=kOutput, calls=%fused_computation.18 | convolution fusion | flops 1075445760 | bytes 6815748 | tf_op jit(solution)/shard_map/dot_general | solution.py:105
  277.6 184.5 %reduce-scatter.2.cloned.1.call-done = bf16[64,2048]{1,0:T(8,128)(2,1)} async-done(((bf16[512,2048]{1,0:T(8,128)(2,1)}), bf16[64,2048]{1,0:T(8,128)(2,1)}) %reduce-scatter.2.cloned.1.call-update) | async-done | bytes 262160 | tf_op jit(solution)/shard_map/reduce_scatter | solution.py:104
  (121 shorter events, 11.0 us)
Async XLA Ops:
  6.5 266.0 %copy-start = (bf16[2048,256]{1,0:T(8,128)(2,1)S(1)}, bf16[2048,256]{1,0:T(8,128)(2,1)}, u32[]{:S(2)}) copy-start(bf16[2048,256]{1,0:T(8,128)(2,1)} %param.16) | copy-start | bytes 3145732
  6.5 33.5 %all-gather.4.cloned.1.call-start = ((), (), s32[]{:S(2)}) async-start(), calls=%async_computation.1 | async-start | bytes 2359296 | tf_op jit(solution)/shard_map/all_gather | solution.py:23
  7.3 176.7 %all-gather.6.cloned.1.call-start = ((), (), s32[]{:S(2)}) async-start(), calls=%async_computation.3 | async-start | bytes 17301504 | tf_op jit(solution)/shard_map/all_gather | solution.py:81
  40.1 2.7 copy-start.1
  40.1 2.8 copy-start.4
  42.9 1.7 copy-start.5
  42.9 1.7 copy-start.3
  44.4 417.7 %reduce-scatter.2.cloned.1.call-start = ((), (), s32[]{:S(2)}) async-start(), calls=%async_computation.2 | async-start | bytes 2359296 | tf_op jit(solution)/shard_map/reduce_scatter | solution.py:104
  268.4 4.1 copy-start.2
Sparse Core Ops, SparseCore 0:
  9.2 30.8 all-gather.3
  44.6 139.3 all-gather.5
  277.8 184.3 reduce-scatter.1
